TPU v7x, 256 devices: a whole 4x4x8 slice. The times are simulated.
256 devices in a mesh: sp: 32 (over z, y), tp: 8 (over x, core).
Axes of the slice: x: 4, y: 4, z: 8, core: 2. Of those that a mesh axis runs over, the one named last changes fastest.
Arguments:
- tokens: bfloat16 [32768, 4096], P('sp', 'tp'), may hold values from -6 to 6
- norm_gain: float32 [4096], replicated, may hold values from 0.1 to 1.9
- pool_in_weight: bfloat16 [4096, 2048], P('sp', 'tp'), may hold values from -0.09375 to 0.09375
- query_weight: bfloat16 [4096, 2048], P('sp', 'tp'), may hold values from -1 to 1, as said below
- key_weight: bfloat16 [4096, 512], P('sp', 'tp'), may hold values from -40 to 40
- value_weight: bfloat16 [4096, 512], P('sp', 'tp'), may hold values from -0.09375 to 0.09375
- pool_weight: bfloat16 [8, 256, 256], P('tp'), may hold values from -0.375 to 0.375
- pool_scale: float32 [2048], P('tp'), may hold values from 0.1 to 1.9
- sink_logit: float32 [32], P('tp'), may hold values from 3 to 7
- out_pool_weight: bfloat16 [2048, 4096], P('tp', 'sp'), may hold values from -0.09375 to 0.09375
- out_attn_weight: bfloat16 [2048, 4096], P('tp', 'sp'), may hold values from -1.5 to 1.5
Outputs:
- mixed: bfloat16 [32768, 4096], P(('sp', 'tp'))
Inputs may be any that keep to these rules, and one draw needn't show every extreme that they name: `query_weight`: entries of order 4096 ** -0.5, drawn independently.
All inputs are finite; a program needn't handle non-finite values.
Results may differ from a plain program's by a relative error of at most 0.014.
The roundings to bfloat16 on the way count: a program that leaves them out, or rounds other values in their place, can miss the bound.
Values may be sent and summed in bfloat16 or wider, within the bound.
No kernel may reach another device: no remote copies, remote signals or barrier semaphores. Data moves between devices by JAX's collectives and lax.ppermute only.
A program may use at most 128 MiB of HBM per device.

v0:
```python
import jax
import jax.numpy as jnp
from jax import lax
from jax.sharding import Mesh
from jax.sharding import PartitionSpec as P

HEAD_DIM = 64
Q_HEADS = 32
KV_HEADS = 8
GROUP_DIM = 256
WINDOW = 128
GRID_W = 64
SP = ("sp_0", "sp_1")
SP_TP = ("sp_0", "sp_1", "tp")
epsilon = 1e-06
rotary_base = 10000.0
masked_score = -1e30


def sent_together(arrays, axis, dim, along):
    widths = [a.shape[along] for a in arrays]
    both = jnp.concatenate(arrays, axis=along)
    result = lax.all_gather(both, axis, axis=dim, tiled=True)
    return tuple(jnp.split(result, [sum(widths[:k]) for k in range(1, len(widths))], axis=along))


def padded_2(block, sides, width):
    for axis, dim in sides:
        count = lax.axis_size(axis)
        forward = [(i, i + 1) for i in range(count - 1)]
        backward = [(target, source) for source, target in forward]
        low = lax.ppermute(
            lax.slice_in_dim(block, block.shape[dim] - width, None, axis=dim), axis, forward
        )
        high = lax.ppermute(lax.slice_in_dim(block, 0, width, axis=dim), axis, backward)
        block = jnp.concatenate([low, block, high], axis=dim)
    return block


def gather_axes(array, axes, dim):
    if not axes:
        return array
    nearer = lax.all_gather(array, axes[-1], axis=dim, tiled=True)
    return gather_axes(nearer, axes[:-1], dim)


def rms_normed(values, gain):
    floats = values.astype(jnp.float32)
    scaled = floats * lax.rsqrt(jnp.mean(floats * floats, axis=-1, keepdims=True) + epsilon)
    return (scaled * gain).astype(jnp.bfloat16)


def rotary_tables(positions, head_dim, grid_width):
    freq_count = head_dim // 4
    inverse = rotary_base ** (-jnp.arange(freq_count, dtype=jnp.float32) / freq_count)
    row_pos = (positions // grid_width).astype(jnp.float32)
    col_pos = (positions % grid_width).astype(jnp.float32)
    angles = jnp.stack([row_pos[:, None] * inverse, col_pos[:, None] * inverse], axis=1)
    return (jnp.cos(angles), jnp.sin(angles))


def rotate(values, cosine, sine):
    length, heads, head_dim = values.shape
    split = values.reshape(length, heads, 2, 2, head_dim // 4)
    first = split[:, :, :, 0]
    second = split[:, :, :, 1]
    cos_b = cosine[:, None]
    sin_b = sine[:, None]
    turned = jnp.stack([first * cos_b - second * sin_b, second * cos_b + first * sin_b], axis=3)
    return turned.reshape(length, heads, head_dim)


def shards(
    tokens,
    norm_gain,
    pool_in_weight,
    query_weight,
    key_weight,
    value_weight,
    pool_weight,
    pool_scale,
    sink_logit,
    out_pool_weight,
    out_attn_weight,
):
    whole_rows = lax.all_gather(tokens, "tp", axis=1, tiled=True)
    normed = rms_normed(whole_rows, norm_gain)
    tok_rows = normed.shape[0]

    def project(piece):
        return jnp.dot(normed, piece, preferred_element_type=jnp.float32)

    pieces = sent_together((pool_in_weight, query_weight, key_weight, value_weight), SP, 0, 1)
    pool_raw, query_raw, key_raw, value_raw = tuple((project(piece) for piece in pieces))
    sp_index = lax.axis_index(SP)
    tp_index = lax.axis_index("tp")
    total_rows = tok_rows * lax.axis_size(SP)
    offset = sp_index * tok_rows
    positions = offset + jnp.arange(tok_rows, dtype=jnp.int32)
    cosine, sine = rotary_tables(positions, HEAD_DIM, GRID_W)
    pool_in = pool_raw.astype(jnp.bfloat16)
    queries = rotate(query_raw.reshape(tok_rows, -1, HEAD_DIM), cosine, sine).astype(jnp.bfloat16)
    key_part = rotate(key_raw.reshape(tok_rows, -1, HEAD_DIM), cosine, sine).astype(jnp.bfloat16)
    key_part = key_part.reshape(tok_rows, -1)
    value_part = value_raw.astype(jnp.bfloat16)
    kv_rows = jnp.concatenate([key_part, value_part], axis=1)
    kv_width = key_part.shape[1]
    channels = pool_in.shape[1]
    pool_reach = 8
    rim_depth = max(WINDOW, pool_reach)
    padded = padded_2(jnp.concatenate([pool_in, kv_rows], axis=1), ((SP, 0),), rim_depth)
    pool_pad = padded[rim_depth - pool_reach : rim_depth + tok_rows + pool_reach, :channels]
    kv_pad = padded[rim_depth - WINDOW : rim_depth + tok_rows + WINDOW, channels:]
    running = jnp.concatenate(
        [jnp.zeros((1, channels), jnp.float32), jnp.cumsum(pool_pad.astype(jnp.float32), axis=0)],
        axis=0,
    )
    groups_dev = channels // GROUP_DIM
    selector = (tp_index * groups_dev + jnp.arange(channels, dtype=jnp.int32) // GROUP_DIM) % 4
    window_mean = jnp.zeros((tok_rows, channels), jnp.float32)
    for level, half_width in enumerate((1, 2, 4, 8)):
        window_sum = (
            running[pool_reach + half_width : pool_reach + half_width + tok_rows]
            - running[pool_reach - half_width : pool_reach - half_width + tok_rows]
        )
        counts = jnp.minimum(positions + half_width, total_rows) - jnp.maximum(
            positions - half_width, 0
        )
        level_mean = window_sum / counts.astype(jnp.float32)[:, None]
        window_mean = jnp.where((selector == level)[None, :], level_mean, window_mean)
    pooled = (window_mean - pool_in.astype(jnp.float32)).astype(jnp.bfloat16)
    mixing = jnp.einsum(
        "tgc,gcd->tgd",
        pooled.reshape(tok_rows, groups_dev, GROUP_DIM),
        pool_weight,
        preferred_element_type=jnp.float32,
    )
    pool_out = (mixing.reshape(tok_rows, channels) * pool_scale).astype(jnp.bfloat16)
    group = Q_HEADS // KV_HEADS
    kv_heads_dev = kv_width // HEAD_DIM
    query_groups = queries.reshape(tok_rows, kv_heads_dev, group, HEAD_DIM)
    key_pad = kv_pad[:, :kv_width].reshape(-1, kv_heads_dev, HEAD_DIM)
    value_pad = kv_pad[:, kv_width:].reshape(-1, kv_heads_dev, HEAD_DIM)
    scores = jnp.einsum(
        "qkgd,skd->kgqs", query_groups, key_pad, preferred_element_type=jnp.float32
    ) * HEAD_DIM ** (-0.5)
    key_pos = offset - WINDOW + jnp.arange(tok_rows + 2 * WINDOW, dtype=jnp.int32)
    allowed = (
        (jnp.abs(key_pos[None, :] - positions[:, None]) <= WINDOW)
        & (key_pos >= 0)[None, :]
        & (key_pos < total_rows)[None, :]
    )
    scores = jnp.where(allowed, scores, masked_score)
    sink = sink_logit.reshape(kv_heads_dev, group, 1, 1)
    highest = jnp.maximum(jnp.max(scores, axis=-1, keepdims=True), sink)
    expo = jnp.exp(scores - highest)
    denominator = jnp.sum(expo, axis=-1, keepdims=True) + jnp.exp(sink - highest)
    weights = (expo / denominator).astype(jnp.bfloat16)
    attended = jnp.einsum("kgqs,skd->qkgd", weights, value_pad, preferred_element_type=jnp.float32)
    attn_out = attended.reshape(tok_rows, -1).astype(jnp.bfloat16)
    out_pool_full, out_attn_full = (
        gather_axes(out_pool_weight, SP, 1),
        gather_axes(out_attn_weight, SP, 1),
    )
    return lax.psum_scatter(
        (
            jnp.dot(pool_out, out_pool_full, preferred_element_type=jnp.float32)
            + jnp.dot(attn_out, out_attn_full, preferred_element_type=jnp.float32)
        ).astype(jnp.bfloat16),
        "tp",
        scatter_dimension=0,
        tiled=True,
    )


def solution(mesh):
    finer = Mesh(mesh.devices.reshape(8, 4, mesh.shape["tp"]), ("sp_0", "sp_1", "tp"))
    return jax.shard_map(
        shards,
        mesh=finer,
        in_specs=(
            P(SP, "tp"),
            P(),
            P(SP, "tp"),
            P(SP, "tp"),
            P(SP, "tp"),
            P(SP, "tp"),
            P("tp", None, None),
            P("tp"),
            P("tp"),
            P("tp", SP),
            P("tp", SP),
        ),
        out_specs=P(SP_TP, None),
        check_vma=False,
    )
```

profile of v0, /device:TPU:1, one launch (start us, length us, event | category | flops | bytes accessed | tf_op | source)
XLA Modules:
  0.0 306.1 jit_solution(10103627928105953874)
XLA Ops:
  9.0 1.6 pad_maximum_fusion.2
  10.7 12.0 %all_gather.20 = bf16[256,512]{1,0:T(8,128)(2,1)} all-gather(bf16[256,128]{1,0:T(8,128)(2,1)} %param.20), channel_id=1, replica_groups=mesh['sp_0'=8,'sp_1'=4,'tp'=8] {'sp_1'}, dimensions={1}, use_global_device_ids=true | all-gather | bytes 327680 | tf_op jit(solution)/shard_map/all_gather | solution.py:43
  22.7 11.1 %all_gather.22 = bf16[256,512]{1,0:T(8,128)(2,1)} all-gather(bf16[256,128]{1,0:T(8,128)(2,1)} %param.21), channel_id=1, replica_groups=mesh['sp_0'=8,'sp_1'=4,'tp'=8] {'sp_1'}, dimensions={1}, use_global_device_ids=true | all-gather | bytes 327680 | tf_op jit(solution)/shard_map/all_gather | solution.py:43
  35.7 3.1 fusion.7
  38.8 26.8 %all-gather.5.cloned.1.call-done = bf16[1024,4096]{1,0:T(8,128)(2,1)} async-done(((bf16[1024,512]{1,0:T(8,128)(2,1)}), bf16[1024,4096]{1,0:T(8,128)(2,1)}) %all-gather.5.cloned.1.call-update) | async-done | bytes 8388624 | tf_op jit(solution)/shard_map/all_gather | solution.py:86
  65.6 5.1 %fusion.1 = f32[1024]{0:T(1024)S(1)} fusion(bf16[1024,4096]{1,0:T(8,128)(2,1)} %all-gather.5.cloned.1.call-done), kind=kLoop, calls=%fused_computation.6 | loop fusion | flops 12581888 | bytes 8392704 | tf_op jit(solution)/shard_map/reduce_sum | solution.py:49
  70.7 10.3 %fusion.3 = bf16[1024,4096]{1,0:T(8,128)(2,1)} fusion(bf16[1024,4096]{1,0:T(8,128)(2,1)} %all-gather.5.cloned.1.call-done, f32[4096]{0:T(1024)S(1)} %copy-done.13, f32[1024]{0:T(1024)S(1)} %add_rsqrt_fusion), kind=kLoop, calls=%fused_computation.8 | loop fusion | flops 16777216 | bytes 16797696 | tf_op jit(solution)/shard_map/convert_element_type | solution.py:50
  81.0 68.8 %all-gather.7.cloned.1.call-done = bf16[4096,640]{1,0:T(8,128)(2,1)} async-done(((bf16[128,640]{1,0:T(8,128)(2,1)}), bf16[4096,640]{1,0:T(8,128)(2,1)}) %all-gather.7.cloned.1.call-update) | async-done | bytes 5242896 | tf_op jit(solution)/shard_map/all_gather | solution.py:23
  149.9 6.4 %fusion.33 = f32[1024,64]{0,1:T(8,128)S(1)} fusion(bf16[1024,4096]{1,0:T(8,128)(2,1)} %fusion.3, bf16[4096,640]{1,0:T(8,128)(2,1)} %all-gather.7.cloned.1.call-done), kind=kOutput, calls=%fused_computation.42 | convolution fusion | flops 536870912 | bytes 9699328 | tf_op jit(solution)/shard_map/dot_general | solution.py:91
  157.4 2.4 fusion.14
  159.8 2.7 convolution_convert_fusion
  162.6 1.9 collective-permute-start
  164.5 1.5 collective-permute-start.1
  166.0 2.4 fusion.8
  171.6 1.3 fusion.12
  173.2 5.2 %fusion.96 = (f32[4,1024]{1,0:T(4,128)S(1)}, f32[1,4,1024,1280]{2,3,1,0:T(8,128)S(1)}) fusion(bf16[1024,4,64]{0,2,1:T(8,128)(2,1)} %bitcast.62, bf16[128,384]{0,1:T(8,128)(2,1)} %copy-done.11, bf16[128,384]{0,1:T(8,128)(2,1)} %copy-done.9, bf16[1024,64]{0,1:T(8,128)(2,1)S(1)} %convolution_convert_fusion, bf16[1024,64]{0,1:T(8,128)(2,1)} %bitcast.59, ...), kind=kOutput, calls=%fused_computation.140 | convolution fusion | flops 687632384 | bytes 23805952 | tf_op jit(solution)/shard_map/qkgd,skd->kgqs/dot_general | solution.py:144
  178.5 3.0 fusion
  181.5 4.0 %copy-done.3 = f32[1,4,1024,1280]{2,3,1,0:T(8,128)} copy-done((f32[1,4,1024,1280]{2,3,1,0:T(8,128)}, f32[1,4,1024,1280]{2,3,1,0:T(8,128)S(1)}, u32[]{:S(2)}) %copy-start.3) | copy-done | bytes 20971544
  186.7 3.0 all-gather.9.cloned.1.call-done
  189.8 10.7 %fusion.21 = f32[1024,4096]{1,0:T(8,128)} fusion(bf16[256,4096]{1,0:T(8,128)(2,1)} %all-gather.9.cloned.1.call-done, bf16[1024,256]{0,1:T(8,128)(2,1)S(1)} %copy-done.5, f32[1152,256]{0,1:T(8,128)S(1)} %bitcast.55, f32[1040,256]{0,1:T(8,128)S(1)} %bitcast.56, f32[256]{0:T(256)S(1)} %copy-done.15, f32[1024]{0:T(1024)S(1)} %get-tuple-element.23, ...), kind=kOutput, calls=%fused_computation.25 | convolution fusion | flops 2286157824 | bytes 28068864 | tf_op jit(solution)/shard_map/dot_general | solution.py:167
  200.5 9.3 %fusion.18 = bf16[64,4,1024]{2,0,1:T(8,128)(2,1)S(1)} fusion(f32[4,1024]{1,0:T(4,128)S(1)} %exponential_add_fusion, f32[1,4,1024,1280]{2,3,1,0:T(8,128)} %copy-done.3, f32[4,1024]{1,0:T(4,128)S(1)} %broadcast_maximum_fusion, bf16[128,384]{0,1:T(8,128)(2,1)S(1)} %copy-done.12, bf16[128,384]{0,1:T(8,128)(2,1)S(1)} %copy-done.10, ...), kind=kOutput, calls=%fused_computation.24 | convolution fusion | flops 687898624 | bytes 22511616 | tf_op jit(solution)/shard_map/kgqs,skd->qkgd/dot_general | solution.py:159
  209.8 20.3 %all-gather.11.cloned.1.call-done = bf16[256,4096]{1,0:T(8,128)(2,1)} async-done(((bf16[256,512]{1,0:T(8,128)(2,1)}), bf16[256,4096]{1,0:T(8,128)(2,1)}) %all-gather.11.cloned.1.call-update) | async-done | bytes 2097168 | tf_op jit(solution)/shard_map/all_gather | solution.py:43
  230.1 12.1 %add_convert_fusion = bf16[1024,4096]{1,0:T(8,128)(2,1)} fusion(f32[1024,4096]{1,0:T(8,128)} %fusion.21, bf16[1024,256]{0,1:T(8,128)(2,1)S(1)} %bitcast.54, bf16[256,4096]{1,0:T(8,128)(2,1)} %all-gather.11.cloned.1.call-done), kind=kOutput, calls=%fused_computation.9 | convolution fusion | flops 2155872256 | bytes 27787264 | tf_op jit(solution)/shard_map/dot_general | solution.py:168
  242.2 57.4 %reduce-scatter.2.cloned.1.call-done = bf16[128,4096]{1,0:T(8,128)(2,1)} async-done(((bf16[1024,4096]{1,0:T(8,128)(2,1)}), bf16[128,4096]{1,0:T(8,128)(2,1)}) %reduce-scatter.2.cloned.1.call-update) | async-done | bytes 1048592 | tf_op jit(solution)/shard_map/reduce_scatter | solution.py:165
  (81 shorter events, 10.3 us)
Async XLA Ops:
  6.5 183.2 %copy-start = (bf16[1,256,256]{2,1,0:T(8,128)(2,1)S(1)}, bf16[1,256,256]{2,1,0:T(8,128)(2,1)}, u32[]{:S(2)}) copy-start(bf16[1,256,256]{2,1,0:T(8,128)(2,1)} %param.17) | copy-start | bytes 393220
  6.5 59.1 %all-gather.5.cloned.1.call-start = ((), (), s32[]{:S(2)}) async-start(), calls=%async_computation.1 | async-start | bytes 9437184 | tf_op jit(solution)/shard_map/all_gather | solution.py:86
  7.3 142.6 %all-gather.7.cloned.1.call-start = ((), (), s32[]{:S(2)}) async-start(), calls=%async_computation.2 | async-start | bytes 5406720 | tf_op jit(solution)/shard_map/all_gather | solution.py:23
  10.6 179.1 %all-gather.9.cloned.1.call-start = ((), (), s32[]{:S(2)}) async-start(), calls=%async_computation.3 | async-start | bytes 2359296 | tf_op jit(solution)/shard_map/all_gather | solution.py:43
  22.7 207.4 %all-gather.11.cloned.1.call-start = ((), (), s32[]{:S(2)}) async-start(), calls=%async_computation.4 | async-start | bytes 2359296 | tf_op jit(solution)/shard_map/all_gather | solution.py:43
  33.8 36.9 %copy-start.13 = (f32[4096]{0:T(1024)S(1)}, f32[4096]{0:T(1024)}, u32[]{:S(2)}) copy-start(f32[4096]{0:T(1024)} %param.12) | copy-start | bytes 49156
  33.8 265.8 %reduce-scatter.2.cloned.1.call-start = ((), (), s32[]{:S(2)}) async-start(), calls=%async_computation.5 | async-start | bytes 9437184 | tf_op jit(solution)/shard_map/reduce_scatter | solution.py:165
  149.8 6.9 %copy-start.2 = (bf16[1024,4096]{1,0:T(8,128)(2,1)S(1)}, bf16[1024,4096]{1,0:T(8,128)(2,1)}, u32[]{:S(2)}) copy-start(bf16[1024,4096]{1,0:T(8,128)(2,1)} %fusion.3) | copy-start | bytes 25165828
  149.9 7.6 %copy-start.8 = (bf16[4096,640]{1,0:T(8,128)(2,1)S(1)}, bf16[4096,640]{1,0:T(8,128)(2,1)}, u32[]{:S(2)}) copy-start(bf16[4096,640]{1,0:T(8,128)(2,1)} %all-gather.7.cloned.1.call-done) | copy-start | bytes 15728644
  157.4 12.8 %copy-start.6 = (bf16[1024,1,2,2,16]{0,4,3,2,1:T(8,128)(2,1)}, bf16[1024,1,2,2,16]{0,4,3,2,1:T(8,128)(2,1)S(1)}, u32[]{:S(2)}) copy-start(bf16[1024,1,2,2,16]{0,4,3,2,1:T(8,128)(2,1)S(1)} %pad_maximum_fusion.4) | copy-start | bytes 393220
  159.8 10.4 %copy-start.4 = (bf16[1024,256]{0,1:T(8,128)(2,1)}, bf16[1024,256]{0,1:T(8,128)(2,1)S(1)}, u32[]{:S(2)}) copy-start(bf16[1024,256]{0,1:T(8,128)(2,1)S(1)} %fusion.14) | copy-start | bytes 1572868
  162.6 6.8 %collective-permute-start = (bf16[128,384]{0,1:T(8,128)(2,1)S(1)}, bf16[128,384]{0,1:T(8,128)(2,1)S(1)}, u32[]{:S(2)}, u32[]{:S(2)}) collective-permute-start(bf16[128,384]{0,1:T(8,128)(2,1)S(1)} %get-tuple-element.7), channel_id=1, source_target_pairs={{0,8},{8,16},{16,24},{24,32},{32,40},{40,48},{48,56},{56,64},{64,7... | collective-permute-start | bytes 294920 | tf_op jit(solution)/shard_map/ppermute | solution.py:32
  164.5 5.8 %collective-permute-start.1 = (bf16[128,384]{0,1:T(8,128)(2,1)S(1)}, bf16[128,384]{0,1:T(8,128)(2,1)S(1)}, u32[]{:S(2)}, u32[]{:S(2)}) collective-permute-start(bf16[128,384]{0,1:T(8,128)(2,1)S(1)} %get-tuple-element.8), channel_id=1, source_target_pairs={{8,0},{16,8},{24,16},{32,24},{40,32},{48,40},{56,48},{64,56},{72,6... | collective-permute-start | bytes 294920 | tf_op jit(solution)/shard_map/ppermute | solution.py:35
  173.2 5.2 %copy-start.14 = (f32[4]{0:T(128)S(1)}, f32[4]{0:T(128)}, u32[]{:S(2)}) copy-start(f32[4]{0:T(128)} %param.19) | copy-start | bytes 52
  178.4 7.1 %copy-start.3 = (f32[1,4,1024,1280]{2,3,1,0:T(8,128)}, f32[1,4,1024,1280]{2,3,1,0:T(8,128)S(1)}, u32[]{:S(2)}) copy-start(f32[1,4,1024,1280]{2,3,1,0:T(8,128)S(1)} %get-tuple-element.20) | copy-start | bytes 62914564
  185.5 4.2 %copy-start.5 = (bf16[1024,256]{0,1:T(8,128)(2,1)S(1)}, bf16[1024,256]{0,1:T(8,128)(2,1)}, u32[]{:S(2)}) copy-start(bf16[1024,256]{0,1:T(8,128)(2,1)} %copy-done.4) | copy-start | bytes 1572868
  185.5 4.2 %copy-start.15 = (f32[256]{0:T(256)S(1)}, f32[256]{0:T(256)}, u32[]{:S(2)}) copy-start(f32[256]{0:T(256)} %param.18) | copy-start | bytes 3076
  185.5 4.2 %copy-start.16 = (pred[256]{0:T(512)(128)(4,1)S(1)}, pred[256]{0:T(512)(128)(4,1)}, u32[]{:S(2)}) copy-start(pred[256]{0:T(512)(128)(4,1)} %get-tuple-element.27) | copy-start | bytes 772
  185.5 4.2 %copy-start.17 = (pred[256]{0:T(512)(128)(4,1)S(1)}, pred[256]{0:T(512)(128)(4,1)}, u32[]{:S(2)}) copy-start(pred[256]{0:T(512)(128)(4,1)} %get-tuple-element.28) | copy-start | bytes 772
  185.6 4.2 %copy-start.18 = (pred[256]{0:T(512)(128)(4,1)S(1)}, pred[256]{0:T(512)(128)(4,1)}, u32[]{:S(2)}) copy-start(pred[256]{0:T(512)(128)(4,1)} %get-tuple-element.29) | copy-start | bytes 772
  189.8 10.7 %copy-start.7 = (bf16[1024,1,2,2,16]{0,4,3,2,1:T(8,128)(2,1)S(1)}, bf16[1024,1,2,2,16]{0,4,3,2,1:T(8,128)(2,1)}, u32[]{:S(2)}) copy-start(bf16[1024,1,2,2,16]{0,4,3,2,1:T(8,128)(2,1)} %copy-done.6) | copy-start | bytes 393220
  189.8 10.7 %copy-start.10 = (bf16[128,384]{0,1:T(8,128)(2,1)S(1)}, bf16[128,384]{0,1:T(8,128)(2,1)}, u32[]{:S(2)}) copy-start(bf16[128,384]{0,1:T(8,128)(2,1)} %copy-done.9) | copy-start | bytes 294916
  189.8 10.7 %copy-start.12 = (bf16[128,384]{0,1:T(8,128)(2,1)S(1)}, bf16[128,384]{0,1:T(8,128)(2,1)}, u32[]{:S(2)}) copy-start(bf16[128,384]{0,1:T(8,128)(2,1)} %copy-done.11) | copy-start | bytes 294916
  230.1 69.5 %copy-start.1 = (bf16[1,256,256]{2,1,0:T(8,128)(2,1)S(1)}, bf16[1,256,256]{2,1,0:T(8,128)(2,1)}, u32[]{:S(2)}) copy-start(bf16[1,256,256]{2,1,0:T(8,128)(2,1)} %param.17) | copy-start | bytes 393220
  (3 other events, 5.8 us)
Sparse Core Ops, SparseCore 0:
  9.2 56.4 all-gather.4
  68.2 81.6 all-gather.6
  151.6 38.0 all-gather.8
  191.4 38.6 all-gather.10
  242.3 57.2 reduce-scatter.1
where the time goes:
time: 307 us; the launch traced here: 306 us
  waiting for transfers between devices  178 us (58%)
  matrix products  51.3 us (17%)
  other arithmetic  28.3 us (9%)
  blocking collectives  23 us (7%)
  between operations  13.5 us (4%)
  local copies, waits for them, and re-layouts  8.52 us (3%)
  starting transfers between devices  3.52 us (1%)
    all_gather x1, waiting for transfers between devices, sent_together(): result = lax.all_gather(both, axis, axis=dim, tiled=True)  68.8 us
    reduce_scatter x1, waiting for transfers between devices, shards(): lax.psum_scatter((jnp.dot(pool_out, out_pool_full, preferred_element_type...  57.4 us
    all_gather x1, waiting for transfers between devices, shards(): whole_rows = lax.all_gather(tokens, 'tp', axis=1, tiled=True)  26.8 us
    all_gather x2, waiting for transfers between devices, gather_axes(): nearer = lax.all_gather(array, axes[-1], axis=dim, tiled=True)  23.3 us
    all_gather x2, blocking collectives, gather_axes(): nearer = lax.all_gather(array, axes[-1], axis=dim, tiled=True)  23 us
    dot_general x4, matrix products, project(): return jnp.dot(normed, piece, preferred_element_type=jnp.float32)  13.9 us
    dot_general x1, matrix products, shards(): jnp.dot(attn_out, out_attn_full, preferred_element_type=jnp.float32)  12.1 us
    dot_general x1, matrix products, shards(): jnp.dot(pool_out, out_pool_full, preferred_element_type=jnp.float32)  10.7 us
  transfers between devices with their start and end apart: 7, of which 6 were waited for; matrix products, arithmetic and copies ran while one was open for 23% of the time, Pallas kernels for 0%

commit v1 on v0

--- a/solution.py
+++ b/solution.py
@@ -15,6 +15,19 @@
 epsilon = 1e-06
 rotary_base = 10000.0
 masked_score = -1e30
+
+
+def gather_around(shard, axis, dim):
+    ways = lax.axis_size(axis)
+    up = [(d, (d + 1) % ways) for d in range(ways)]
+    down = [(d, (d - 1) % ways) for d in range(ways)]
+    earlier, later = ([shard], [shard])
+    for _ in range(ways // 2):
+        earlier.append(lax.ppermute(earlier[-1], axis, up))
+    for _ in range((ways - 1) // 2):
+        later.append(lax.ppermute(later[-1], axis, down))
+    line = jnp.concatenate([*earlier[::-1], *later[1:]], axis=dim)
+    return jnp.roll(line, (lax.axis_index(axis) - ways // 2) * shard.shape[dim], axis=dim)
 
 
 def sent_together(arrays, axis, dim, along):
@@ -83,7 +96,7 @@
     out_pool_weight,
     out_attn_weight,
 ):
-    whole_rows = lax.all_gather(tokens, "tp", axis=1, tiled=True)
+    whole_rows = gather_around(tokens, "tp", 1)
     normed = rms_normed(whole_rows, norm_gain)
     tok_rows = normed.shape[0]
 

time: 307 us -> 261 us (0.85)
  waiting for transfers between devices: 178 us -> 93.3 us
  local copies, waits for them, and re-layouts: 8.52 us -> 32 us
  starting transfers between devices: 3.52 us -> 22.5 us
  other arithmetic: 28.3 us -> 18.3 us
  matrix products: 51.3 us -> 56.1 us
    all_gather x1, waiting for transfers between devices: 68.8 us -> 0.02 us  [sent_together(): result = lax.all_gather(both, axis, axis=dim, tiled=True)]
    ppermute x0 -> x7, waiting for transfers between devices: none -> 31.3 us  [the longest x4 22.9 us: gather_around(): earlier.append(lax.ppermute(earlier[-1], axis, up))]
    all_gather x1 -> x0, waiting for transfers between devices: 26.8 us -> none  [shards(): whole_rows = lax.all_gather(tokens, 'tp', axis=1, tiled=True)]
    unnamed x42 -> x61, local copies, waits for them, and re-layouts: 6.85 us -> 30.2 us
    all_gather x2, waiting for transfers between devices: 23.3 us -> 0.04 us  [gather_axes(): nearer = lax.all_gather(array, axes[-1], axis=dim, tiled=True)]
    ppermute x0 -> x7, starting transfers between devices: none -> 16.9 us  [the longest x4 8.61 us: gather_around(): earlier.append(lax.ppermute(earlier[-1], axis, up))]
    convert_element_type x1 -> x0, other arithmetic: 10.3 us -> none  [rms_normed(): return (scaled * gain).astype(jnp.bfloat16)]
    dot_general x4, matrix products: 13.9 us -> 18.9 us  [project(): return jnp.dot(normed, piece, preferred_element_type=jnp.float32)]
  transfers between devices with their start and end apart: 7 -> 13, of which waited for: 6 -> 5; matrix products, arithmetic and copies ran while one was open for 23% -> 29% of each run, Pallas kernels for 0% -> 0%
where the time goes in v1:
time: 261 us; the launch traced here: 260 us
  waiting for transfers between devices  93.3 us (36%)
  matrix products  56.1 us (21%)
  local copies, waits for them, and re-layouts  32 us (12%)
  blocking collectives  24 us (9%)
  starting transfers between devices  22.5 us (9%)
  other arithmetic  18.3 us (7%)
  between operations  13.8 us (5%)
    reduce_scatter x1, waiting for transfers between devices, shards(): lax.psum_scatter((jnp.dot(pool_out, out_pool_full, preferred_element_type...  61.8 us
    unnamed x61, local copies, waits for them, and re-layouts  30.2 us
    all_gather x2, blocking collectives, gather_axes(): nearer = lax.all_gather(array, axes[-1], axis=dim, tiled=True)  24 us
    ppermute x4, waiting for transfers between devices, gather_around(): earlier.append(lax.ppermute(earlier[-1], axis, up))  22.9 us
    dot_general x4, matrix products, project(): return jnp.dot(normed, piece, preferred_element_type=jnp.float32)  18.9 us
    dot_general x1, matrix products, shards(): jnp.dot(attn_out, out_attn_full, preferred_element_type=jnp.float32)  12.1 us
    dot_general x1, matrix products, shards(): jnp.dot(pool_out, out_pool_full, preferred_element_type=jnp.float32)  10.7 us
    dot_general x1, matrix products, shards(): jnp.einsum('kgqs,skd->qkgd', weights, value_pad, preferred_element_type=j...  9.31 us
  transfers between devices with their start and end apart: 13, of which 5 were waited for; matrix products, arithmetic and copies ran while one was open for 29% of the time, Pallas kernels for 0%

profile of v1, /device:TPU:1, one launch (start us, length us, event | category | flops | bytes accessed | tf_op | source)
XLA Modules:
  0.0 259.9 jit_solution(14632971366734640196)
XLA Ops:
  10.0 12.0 %all_gather.16 = bf16[256,512]{1,0:T(8,128)(2,1)} all-gather(bf16[256,128]{1,0:T(8,128)(2,1)} %param.20), channel_id=1, replica_groups=mesh['sp_0'=8,'sp_1'=4,'tp'=8] {'sp_1'}, dimensions={1}, use_global_device_ids=true | all-gather | bytes 327680 | tf_op jit(solution)/shard_map/all_gather | solution.py:56
  22.1 3.6 %collective-permute-start = (bf16[1024,512]{1,0:T(8,128)(2,1)}, bf16[1024,512]{1,0:T(8,128)(2,1)S(1)}, u32[]{:S(2)}, u32[]{:S(2)}) collective-permute-start(bf16[1024,512]{1,0:T(8,128)(2,1)} %param.11), channel_id=1, source_target_pairs={{0,1},{1,2},{2,3},{3,4},{4,5},{5,6},{6,7},{7,0},{8,9},{9,10},{10,1... | collective-permute-start | bytes 3145736 | tf_op jit(solution)/shard_map/ppermute | solution.py:26
  25.7 12.1 %collective-permute-done = bf16[1024,512]{1,0:T(8,128)(2,1)S(1)} collective-permute-done((bf16[1024,512]{1,0:T(8,128)(2,1)}, bf16[1024,512]{1,0:T(8,128)(2,1)S(1)}, u32[]{:S(2)}, u32[]{:S(2)}) %collective-permute-start) | collective-permute-done | bytes 1048608 | tf_op jit(solution)/shard_map/ppermute | solution.py:26
  41.1 10.8 %collective-permute-done.1 = bf16[1024,512]{1,0:T(8,128)(2,1)} collective-permute-done((bf16[1024,512]{1,0:T(8,128)(2,1)S(1)}, bf16[1024,512]{1,0:T(8,128)(2,1)}, u32[]{:S(2)}, u32[]{:S(2)}) %collective-permute-start.1) | collective-permute-done | bytes 1048608 | tf_op jit(solution)/shard_map/ppermute | solution.py:26
  51.9 2.6 collective-permute-start.2
  54.5 12.0 %all_gather.18 = bf16[256,512]{1,0:T(8,128)(2,1)} all-gather(bf16[256,128]{1,0:T(8,128)(2,1)} %param.21), channel_id=1, replica_groups=mesh['sp_0'=8,'sp_1'=4,'tp'=8] {'sp_1'}, dimensions={1}, use_global_device_ids=true | all-gather | bytes 327680 | tf_op jit(solution)/shard_map/all_gather | solution.py:56
  68.5 4.6 %collective-permute-start.5 = (bf16[1024,512]{1,0:T(8,128)(2,1)S(1)}, bf16[1024,512]{1,0:T(8,128)(2,1)}, u32[]{:S(2)}, u32[]{:S(2)}) collective-permute-start(bf16[1024,512]{1,0:T(8,128)(2,1)S(1)} %collective-permute-done.4), channel_id=1, source_target_pairs={{0,7},{1,0},{2,1},{3,2},{4,3},{5,4},{6,5},{7,6},{8,15},{9,8},{10,9... | collective-permute-start | bytes 3145736 | tf_op jit(solution)/shard_map/ppermute | solution.py:28
  75.5 3.8 %fusion.7 = pred[1024,1280]{0,1:T(8,128)(4,1)} fusion(s32[1024]{0:T(1024)S(1)} %iota_add_fusion.1, s32[1280]{0:T(1024)S(1)} %iota_add_fusion, pred[1280]{0:T(1024)(128)(4,1)S(1)} %get-tuple-element.31, pred[1280]{0:T(1024)(128)(4,1)} %get-tuple-element.32), kind=kLoop, calls=%fused_computation.14 | loop fusion | flops 6553600 | bytes 1322496 | tf_op jit(solution)/shard_map/and | solution.py:162
  79.3 4.1 %collective-permute-done.5 = bf16[1024,512]{1,0:T(8,128)(2,1)} collective-permute-done((bf16[1024,512]{1,0:T(8,128)(2,1)S(1)}, bf16[1024,512]{1,0:T(8,128)(2,1)}, u32[]{:S(2)}, u32[]{:S(2)}) %collective-permute-start.5) | collective-permute-done | bytes 1048608 | tf_op jit(solution)/shard_map/ppermute | solution.py:28
  83.3 2.7 %collective-permute-start.6 = (bf16[1024,512]{1,0:T(8,128)(2,1)}, bf16[1024,512]{1,0:T(8,128)(2,1)S(1)}, u32[]{:S(2)}, u32[]{:S(2)}) collective-permute-start(bf16[1024,512]{1,0:T(8,128)(2,1)} %collective-permute-done.5), channel_id=1, source_target_pairs={{0,7},{1,0},{2,1},{3,2},{4,3},{5,4},{6,5},{7,6},{8,15},{9,8},{10,9... | collective-permute-start | bytes 3145736 | tf_op jit(solution)/shard_map/ppermute | solution.py:28
  93.8 4.4 %collective-permute-done.6 = bf16[1024,512]{1,0:T(8,128)(2,1)S(1)} collective-permute-done((bf16[1024,512]{1,0:T(8,128)(2,1)}, bf16[1024,512]{1,0:T(8,128)(2,1)S(1)}, u32[]{:S(2)}, u32[]{:S(2)}) %collective-permute-start.6) | collective-permute-done | bytes 1048608 | tf_op jit(solution)/shard_map/ppermute | solution.py:28
  104.3 5.8 %copy-done.2 = bf16[1024,8192]{1,0:T(8,128)(2,1)} copy-done((bf16[1024,8192]{1,0:T(8,128)(2,1)}, bf16[1024,8192]{1,0:T(8,128)(2,1)S(1)}, u32[]{:S(2)}) %copy-start.2) | copy-done | bytes 16777240
  111.9 5.9 %fusion.33 = f32[1024,64]{0,1:T(8,128)S(1)} fusion(bf16[4096,640]{1,0:T(8,128)(2,1)} %all-gather.4.cloned.1.call-done, f32[4096]{0:T(1024)S(1)} %copy-done.21, f32[1024]{0:T(1024)S(1)} %add_rsqrt_fusion, bf16[1024,8192]{1,0:T(8,128)(2,1)} %copy-done.2, s32[]{:T(128)S(6)} %select_n.89), kind=kOutput, calls=%fused_computation.42 | convolution fusion | flops 553648128 | bytes 9719812 | tf_op jit(solution)/shard_map/dot_general | solution.py:104
  120.6 4.1 %convolution_convert_fusion = bf16[1024,64]{0,1:T(8,128)(2,1)S(1)} fusion(bf16[4096,640]{1,0:T(8,128)(2,1)} %all-gather.4.cloned.1.call-done, f32[4096]{0:T(1024)S(1)} %copy-done.21, f32[1024]{0:T(1024)S(1)} %add_rsqrt_fusion, bf16[1024,8192]{1,0:T(8,128)(2,1)S(1)} %copy-done.3, s32[]{:T(128)S(6)} %select_n.89), kind=kOutput, calls=%fused_computation.27 | convolution fusion | flops 553713664 | bytes 9588740 | tf_op jit(solution)/shard_map/dot_general | solution.py:104
  124.7 4.5 %fusion.14 = bf16[1024,256]{0,1:T(8,128)(2,1)S(1)} fusion(bf16[4096,640]{1,0:T(8,128)(2,1)} %all-gather.4.cloned.1.call-done, f32[4096]{0:T(1024)S(1)} %copy-done.21, f32[1024]{0:T(1024)S(1)} %add_rsqrt_fusion, bf16[1024,8192]{1,0:T(8,128)(2,1)S(1)} %copy-done.3, s32[]{:T(128)S(6)} %select_n.89), kind=kOutput, calls=%fused_computation.22 | convolution fusion | flops 2164523008 | bytes 11030532 | tf_op jit(solution)/shard_map/dot_general | solution.py:104
  129.3 4.0 %collective-permute-start.7 = (bf16[128,384]{0,1:T(8,128)(2,1)S(1)}, bf16[128,384]{0,1:T(8,128)(2,1)S(1)}, u32[]{:S(2)}, u32[]{:S(2)}) collective-permute-start(bf16[128,384]{0,1:T(8,128)(2,1)S(1)} %get-tuple-element.7), channel_id=1, source_target_pairs={{0,8},{8,16},{16,24},{24,32},{32,40},{40,48},{48,56},{56,64},{64,7... | collective-permute-start | bytes 294920 | tf_op jit(solution)/shard_map/ppermute | solution.py:45
  134.7 4.4 %fusion.8 = f32[1024,256]{0,1:T(8,128)S(1)} fusion(bf16[4096,640]{1,0:T(8,128)(2,1)} %all-gather.4.cloned.1.call-done, f32[4096]{0:T(1024)S(1)} %copy-done.21, f32[1024]{0:T(1024)S(1)} %add_rsqrt_fusion, bf16[1024,8192]{1,0:T(8,128)(2,1)S(1)} %copy-done.3, s32[]{:T(128)S(6)} %select_n.89), kind=kOutput, calls=%fused_computation.15 | convolution fusion | flops 2164260864 | bytes 11554820 | tf_op jit(solution)/shard_map/dot_general | solution.py:104
  142.8 5.1 %fusion.100 = (f32[4,1024]{1,0:T(4,128)S(1)}, f32[1,4,1024,1280]{2,3,1,0:T(8,128)S(1)}) fusion(bf16[1024,4,64]{0,2,1:T(8,128)(2,1)} %bitcast.57, bf16[128,384]{0,1:T(8,128)(2,1)} %copy-done.14, bf16[128,384]{0,1:T(8,128)(2,1)} %copy-done.12, bf16[1024,64]{0,1:T(8,128)(2,1)} %copy-done.8, bf16[1024,64]{0,1:T(8,128)(2,1)S(1)} %bitcast.54, ...), kind=kOutput, calls=%fused_computation.156 | convolution fusion | flops 687632384 | bytes 23805952 | tf_op jit(solution)/shard_map/qkgd,skd->kgqs/dot_general | solution.py:157
  148.1 7.1 %copy-done.1 = f32[1,4,1024,1280]{2,3,1,0:T(8,128)} copy-done((f32[1,4,1024,1280]{2,3,1,0:T(8,128)}, f32[1,4,1024,1280]{2,3,1,0:T(8,128)S(1)}, u32[]{:S(2)}) %copy-start.1) | copy-done | bytes 20971544
  155.2 2.9 %fusion = f32[4,1024]{1,0:T(4,128)S(1)} fusion(f32[1,4,1024,1280]{2,3,1,0:T(8,128)S(1)} %get-tuple-element.20, f32[4,1024]{1,0:T(4,128)S(1)} %broadcast_maximum_fusion), kind=kLoop, calls=%fused_computation.5 | loop fusion | flops 10481664 | bytes 21004288 | tf_op jit(solution)/shard_map/reduce_sum | solution.py:170
  159.4 10.7 %fusion.21 = f32[1024,4096]{1,0:T(8,128)} fusion(bf16[256,4096]{1,0:T(8,128)(2,1)} %all-gather.6.cloned.1.call-done, bf16[1024,256]{0,1:T(8,128)(2,1)S(1)} %copy-done.6, f32[1152,256]{0,1:T(8,128)S(1)} %bitcast.50, f32[1040,256]{0,1:T(8,128)S(1)} %bitcast.51, f32[256]{0:T(256)} %param.18, f32[1024]{0:T(1024)S(1)} %copy-done.16, f32[1024]{0:T(1024)S(1)} %copy-done.17, ...), kind=kOutput, calls=%fused_computation.25 | convolution fusion | flops 2286157824 | bytes 28067840 | tf_op jit(solution)/shard_map/dot_general | solution.py:180
  170.1 9.3 %fusion.18 = bf16[64,4,1024]{2,0,1:T(8,128)(2,1)S(1)} fusion(f32[4,1024]{1,0:T(4,128)S(1)} %exponential_add_fusion, f32[1,4,1024,1280]{2,3,1,0:T(8,128)} %copy-done.1, f32[4,1024]{1,0:T(4,128)S(1)} %broadcast_maximum_fusion, bf16[128,384]{0,1:T(8,128)(2,1)S(1)} %copy-done.15, bf16[128,384]{0,1:T(8,128)(2,1)S(1)} %copy-done.13, ...), kind=kOutput, calls=%fused_computation.24 | convolution fusion | flops 687898624 | bytes 22511616 | tf_op jit(solution)/shard_map/kgqs,skd->qkgd/dot_general | solution.py:172
  179.4 12.1 %add_convert_fusion = bf16[1024,4096]{1,0:T(8,128)(2,1)} fusion(f32[1024,4096]{1,0:T(8,128)} %fusion.21, bf16[1024,256]{0,1:T(8,128)(2,1)S(1)} %bitcast.49, bf16[256,4096]{1,0:T(8,128)(2,1)} %all-gather.8.cloned.1.call-done), kind=kOutput, calls=%fused_computation.9 | convolution fusion | flops 2155872256 | bytes 27787264 | tf_op jit(solution)/shard_map/dot_general | solution.py:181
  191.6 61.8 %reduce-scatter.2.cloned.1.call-done = bf16[128,4096]{1,0:T(8,128)(2,1)} async-done(((bf16[1024,4096]{1,0:T(8,128)(2,1)}), bf16[128,4096]{1,0:T(8,128)(2,1)}) %reduce-scatter.2.cloned.1.call-update) | async-done | bytes 1048592 | tf_op jit(solution)/shard_map/reduce_scatter | solution.py:178
  (111 shorter events, 35.8 us)
Async XLA Ops:
  6.5 152.8 %copy-start = (bf16[1,256,256]{2,1,0:T(8,128)(2,1)S(1)}, bf16[1,256,256]{2,1,0:T(8,128)(2,1)}, u32[]{:S(2)}) copy-start(bf16[1,256,256]{2,1,0:T(8,128)(2,1)} %param.17) | copy-start | bytes 393220
  6.5 96.0 %copy-start.4 = (bf16[1024,512]{1,0:T(8,128)(2,1)S(1)}, bf16[1024,512]{1,0:T(8,128)(2,1)}, u32[]{:S(2)}) copy-start(bf16[1024,512]{1,0:T(8,128)(2,1)} %param.11) | copy-start | bytes 3145732
  6.5 105.3 %all-gather.4.cloned.1.call-start = ((), (), s32[]{:S(2)}) async-start(), calls=%async_computation.1 | async-start | bytes 5406720 | tf_op jit(solution)/shard_map/all_gather | solution.py:36
  10.0 149.4 %all-gather.6.cloned.1.call-start = ((), (), s32[]{:S(2)}) async-start(), calls=%async_computation.2 | async-start | bytes 2359296 | tf_op jit(solution)/shard_map/all_gather | solution.py:56
  22.0 157.4 %all-gather.8.cloned.1.call-start = ((), (), s32[]{:S(2)}) async-start(), calls=%async_computation.3 | async-start | bytes 2359296 | tf_op jit(solution)/shard_map/all_gather | solution.py:56
  22.1 15.7 %collective-permute-start = (bf16[1024,512]{1,0:T(8,128)(2,1)}, bf16[1024,512]{1,0:T(8,128)(2,1)S(1)}, u32[]{:S(2)}, u32[]{:S(2)}) collective-permute-start(bf16[1024,512]{1,0:T(8,128)(2,1)} %param.11), channel_id=1, source_target_pairs={{0,1},{1,2},{2,3},{3,4},{4,5},{5,6},{6,7},{7,0},{8,9},{9,10},{10,1... | collective-permute-start | bytes 3145736 | tf_op jit(solution)/shard_map/ppermute | solution.py:26
  37.8 14.1 %collective-permute-start.1 = (bf16[1024,512]{1,0:T(8,128)(2,1)S(1)}, bf16[1024,512]{1,0:T(8,128)(2,1)}, u32[]{:S(2)}, u32[]{:S(2)}) collective-permute-start(bf16[1024,512]{1,0:T(8,128)(2,1)S(1)} %collective-permute-done), channel_id=1, source_target_pairs={{0,1},{1,2},{2,3},{3,4},{4,5},{5,6},{6,7},{7,0},{8,9},{9,10},{10,1... | collective-permute-start | bytes 3145736 | tf_op jit(solution)/shard_map/ppermute | solution.py:26
  40.2 28.4 %collective-permute-start.4 = (bf16[1024,512]{1,0:T(8,128)(2,1)}, bf16[1024,512]{1,0:T(8,128)(2,1)S(1)}, u32[]{:S(2)}, u32[]{:S(2)}) collective-permute-start(bf16[1024,512]{1,0:T(8,128)(2,1)} %param.11), channel_id=1, source_target_pairs={{0,7},{1,0},{2,1},{3,2},{4,3},{5,4},{6,5},{7,6},{8,15},{9,8},{10,9... | collective-permute-start | bytes 3145736 | tf_op jit(solution)/shard_map/ppermute | solution.py:28
  51.9 21.3 %collective-permute-start.2 = (bf16[1024,512]{1,0:T(8,128)(2,1)}, bf16[1024,512]{1,0:T(8,128)(2,1)}, u32[]{:S(2)}, u32[]{:S(2)}) collective-permute-start(bf16[1024,512]{1,0:T(8,128)(2,1)} %collective-permute-done.1), channel_id=1, source_target_pairs={{0,1},{1,2},{2,3},{3,4},{4,5},{5,6},{6,7},{7,0},{8,9},{9,10},{10,1... | collective-permute-start | bytes 3145736 | tf_op jit(solution)/shard_map/ppermute | solution.py:26
  66.5 186.9 %reduce-scatter.2.cloned.1.call-start = ((), (), s32[]{:S(2)}) async-start(), calls=%async_computation.4 | async-start | bytes 9437184 | tf_op jit(solution)/shard_map/reduce_scatter | solution.py:178
  68.5 14.8 %collective-permute-start.5 = (bf16[1024,512]{1,0:T(8,128)(2,1)S(1)}, bf16[1024,512]{1,0:T(8,128)(2,1)}, u32[]{:S(2)}, u32[]{:S(2)}) collective-permute-start(bf16[1024,512]{1,0:T(8,128)(2,1)S(1)} %collective-permute-done.4), channel_id=1, source_target_pairs={{0,7},{1,0},{2,1},{3,2},{4,3},{5,4},{6,5},{7,6},{8,15},{9,8},{10,9... | collective-permute-start | bytes 3145736 | tf_op jit(solution)/shard_map/ppermute | solution.py:28
  73.2 13.5 %collective-permute-start.3 = (bf16[1024,512]{1,0:T(8,128)(2,1)}, bf16[1024,512]{1,0:T(8,128)(2,1)}, u32[]{:S(2)}, u32[]{:S(2)}) collective-permute-start(bf16[1024,512]{1,0:T(8,128)(2,1)} %collective-permute-done.2), channel_id=1, source_target_pairs={{0,1},{1,2},{2,3},{3,4},{4,5},{5,6},{6,7},{7,0},{8,9},{9,10},{10,1... | collective-permute-start | bytes 3145736 | tf_op jit(solution)/shard_map/ppermute | solution.py:26
  83.3 14.8 %collective-permute-start.6 = (bf16[1024,512]{1,0:T(8,128)(2,1)}, bf16[1024,512]{1,0:T(8,128)(2,1)S(1)}, u32[]{:S(2)}, u32[]{:S(2)}) collective-permute-start(bf16[1024,512]{1,0:T(8,128)(2,1)} %collective-permute-done.5), channel_id=1, source_target_pairs={{0,7},{1,0},{2,1},{3,2},{4,3},{5,4},{6,5},{7,6},{8,15},{9,8},{10,9... | collective-permute-start | bytes 3145736 | tf_op jit(solution)/shard_map/ppermute | solution.py:28
  90.9 20.9 %copy-start.21 = (f32[4096]{0:T(1024)S(1)}, f32[4096]{0:T(1024)}, u32[]{:S(2)}) copy-start(f32[4096]{0:T(1024)} %param.12) | copy-start | bytes 49156
  104.2 13.6 %copy-start.10 = (f32[1024,1,1,1,16]{0,4,3,2,1:T(8,128)S(1)}, f32[1024,1,1,1,16]{0,4,3,2,1:T(8,128)}, u32[]{:S(2)}) copy-start(f32[1024,1,1,1,16]{0,4,3,2,1:T(8,128)} %get-tuple-element.14) | copy-start | bytes 196612
  104.2 13.6 %copy-start.11 = (f32[1024,1,1,1,16]{0,4,3,2,1:T(8,128)S(1)}, f32[1024,1,1,1,16]{0,4,3,2,1:T(8,128)}, u32[]{:S(2)}) copy-start(f32[1024,1,1,1,16]{0,4,3,2,1:T(8,128)} %get-tuple-element.17) | copy-start | bytes 196612
  124.7 15.5 %copy-start.8 = (bf16[1024,64]{0,1:T(8,128)(2,1)}, bf16[1024,64]{0,1:T(8,128)(2,1)S(1)}, u32[]{:S(2)}) copy-start(bf16[1024,64]{0,1:T(8,128)(2,1)S(1)} %convolution_convert_fusion) | copy-start | bytes 393220
  129.3 10.9 %collective-permute-start.7 = (bf16[128,384]{0,1:T(8,128)(2,1)S(1)}, bf16[128,384]{0,1:T(8,128)(2,1)S(1)}, u32[]{:S(2)}, u32[]{:S(2)}) collective-permute-start(bf16[128,384]{0,1:T(8,128)(2,1)S(1)} %get-tuple-element.7), channel_id=1, source_target_pairs={{0,8},{8,16},{16,24},{24,32},{32,40},{40,48},{48,56},{56,64},{64,7... | collective-permute-start | bytes 294920 | tf_op jit(solution)/shard_map/ppermute | solution.py:45
  133.2 6.9 %collective-permute-start.8 = (bf16[128,384]{0,1:T(8,128)(2,1)S(1)}, bf16[128,384]{0,1:T(8,128)(2,1)S(1)}, u32[]{:S(2)}, u32[]{:S(2)}) collective-permute-start(bf16[128,384]{0,1:T(8,128)(2,1)S(1)} %get-tuple-element.8), channel_id=1, source_target_pairs={{8,0},{16,8},{24,16},{32,24},{40,32},{48,40},{56,48},{64,56},{72,6... | collective-permute-start | bytes 294920 | tf_op jit(solution)/shard_map/ppermute | solution.py:48
  148.0 11.4 %copy-start.6 = (bf16[1024,256]{0,1:T(8,128)(2,1)S(1)}, bf16[1024,256]{0,1:T(8,128)(2,1)}, u32[]{:S(2)}) copy-start(bf16[1024,256]{0,1:T(8,128)(2,1)} %copy-done.5) | copy-start | bytes 1572868
  148.0 11.4 %copy-start.16 = (f32[1024]{0:T(1024)S(1)}, f32[1024]{0:T(1024)}, u32[]{:S(2)}) copy-start(f32[1024]{0:T(1024)} %get-tuple-element.27) | copy-start | bytes 12292
  158.2 11.9 %copy-start.9 = (bf16[1024,64]{0,1:T(8,128)(2,1)S(1)}, bf16[1024,64]{0,1:T(8,128)(2,1)}, u32[]{:S(2)}) copy-start(bf16[1024,64]{0,1:T(8,128)(2,1)} %copy-done.8) | copy-start | bytes 393220
  158.2 11.9 %copy-start.13 = (bf16[128,384]{0,1:T(8,128)(2,1)S(1)}, bf16[128,384]{0,1:T(8,128)(2,1)}, u32[]{:S(2)}) copy-start(bf16[128,384]{0,1:T(8,128)(2,1)} %copy-done.12) | copy-start | bytes 294916
  158.2 11.9 %copy-start.15 = (bf16[128,384]{0,1:T(8,128)(2,1)S(1)}, bf16[128,384]{0,1:T(8,128)(2,1)}, u32[]{:S(2)}) copy-start(bf16[128,384]{0,1:T(8,128)(2,1)} %copy-done.14) | copy-start | bytes 294916
  (11 other events, 83.6 us)
Sparse Core Ops, SparseCore 0:
  10.1 87.7 all-gather.3
  99.7 35.3 all-gather.5
  136.9 39.3 all-gather.7
  191.7 61.6 reduce-scatter.1
